TPU v7x, 32 devices: a whole 2x2x4 slice. The times are simulated.
32 devices in a mesh: grp: 2 (over y), sp: 4 (over z), tp: 4 (over x, core).
Axes of the slice: x: 2, y: 2, z: 4, core: 2. Of those that a mesh axis runs over, the one named last changes fastest.
Arguments:
- conv_input: bfloat16 [4096, 1024], P(('grp', 'sp'), 'tp'), parts along dimension 0, may hold values from -6 to 6
- pre_gate: bfloat16 [4096, 1024], P(('grp', 'sp'), 'tp'), parts along dimension 0, may hold values from -6 to 6
- post_gate: bfloat16 [4096, 1024], P(('grp', 'sp'), 'tp'), parts along dimension 0, may hold values from -6 to 6
- conv_taps: float32 [3, 1024], replicated, may hold values from -3.5 to 3.5
- out_proj: bfloat16 [1024, 2048], replicated, may hold values from -0.1875 to 0.1875
- residual_in: bfloat16 [4096, 2048], P(('grp', 'sp', 'tp')), parts along dimension 0, may hold values from -6 to 6
- norm_gain: float32 [2048], replicated, may hold values from 0.1 to 1.9
- routes: int32 [4096, 2], P(('grp', 'sp', 'tp')), parts along dimension 0, may hold values from 0 to 7, as said below
- route_weight: float32 [4096, 2], P(('grp', 'sp', 'tp')), parts along dimension 0, may hold values from 0.1 to 1
- w_gate: bfloat16 [8, 2048, 1024], P('sp', None, 'tp'), may hold values from -0.125 to 0.125
- w_up: bfloat16 [8, 2048, 1024], P('sp', None, 'tp'), may hold values from -0.125 to 0.125
- w_down: bfloat16 [8, 1024, 2048], P('sp', 'tp'), may hold values from -0.1875 to 0.1875
Outputs:
- layer_out: bfloat16 [4096, 2048], P(('grp', 'sp', 'tp')), parts along dimension 0
There are 2 independent parts, one for each index of `grp`. A program takes and returns all parts, laid end to end along the dimension named above; an argument that names none is the same for every part. Nothing has to cross between parts.
Inputs may be any that keep to these rules, and one draw needn't show every extreme that they name: `routes`: the two numbers of a row differ and lie in the same group of 2 consecutive experts. In each aligned block of 128 rows every expert is named exactly 32 times.
All inputs are finite; a program needn't handle non-finite values.
Results may differ from a plain program's by a relative error of at most 0.0085.
Values may be sent and summed in bfloat16 or wider, within the bound.
No kernel may reach another device: no remote copies, remote signals or barrier semaphores. Data moves between devices by JAX's collectives and lax.ppermute only.
A program may use at most 64 MiB of HBM per device.

v0:
```python
import jax
import jax.numpy as jnp
from jax import lax
from jax.sharding import PartitionSpec as P

GROUPS = 4
LANES = 128


def shifted(block, axis, distance):
    devices = range(lax.axis_size(axis))
    route = [(i - distance, i) for i in devices if i - distance in devices]
    return lax.ppermute(block, axis, route)


def flipped(block, axis, bit):
    return lax.ppermute(block, axis, [(i, i ^ bit) for i in range(lax.axis_size(axis))])


def mix(conv_input, pre_gate, post_gate, conv_taps):
    channels = conv_input.shape[1]
    taps = lax.dynamic_slice_in_dim(conv_taps, lax.axis_index("tp") * channels, channels, 1)
    edge = jnp.concatenate([conv_input[-2:], pre_gate[-2:]], axis=1)
    prior = shifted(edge, "sp", 1)
    prior_input, prior_gate = (prior[:, :channels], prior[:, channels:])
    gated = jnp.concatenate(
        [
            prior_gate.astype(jnp.float32) * prior_input.astype(jnp.float32),
            pre_gate.astype(jnp.float32) * conv_input.astype(jnp.float32),
        ],
        axis=0,
    )
    conv = gated[2:] * taps[2] + gated[1:-1] * taps[1] + gated[:-2] * taps[0]
    return (post_gate.astype(jnp.float32) * conv).astype(jnp.bfloat16)


def project(mixed, out_proj, residual_in, norm_gain):
    token_rows = lax.all_to_all(mixed, "tp", split_axis=0, concat_axis=1, tiled=True)
    projected = jnp.dot(token_rows, out_proj, preferred_element_type=jnp.float32)
    stream = residual_in.astype(jnp.float32) + projected
    scale = lax.rsqrt(jnp.mean(stream * stream, axis=-1, keepdims=True) + 1e-06)
    normed = (stream * scale * norm_gain).astype(jnp.bfloat16)
    return (stream, normed)


def route_by_group(stream, normed, routes, route_weight, w_gate, w_up, w_down):
    shards = lax.axis_size("tp")
    seq_ranks = lax.axis_size("sp")
    block_rows, width = stream.shape
    local_experts = w_gate.shape[0]
    capacity = block_rows // seq_ranks
    group = routes[:, 0] // local_experts
    order = jnp.arange(block_rows, dtype=jnp.int32)
    earlier = (group[:, None] == group[None, :]) & (order[None, :] < order[:, None])
    slot = group * capacity + jnp.sum(earlier.astype(jnp.int32), axis=1)
    select = (order[:, None] == slot[None, :]).astype(jnp.bfloat16)
    member = routes[:, :, None] % local_experts == jnp.arange(local_experts, dtype=jnp.int32)
    weight = jnp.sum(jnp.where(member, route_weight[:, :, None], 0.0), axis=1)
    high = lax.reduce_precision(weight, 8, 7)
    labels = jnp.concatenate([high, weight - high], axis=1).astype(jnp.bfloat16)
    labels = jnp.pad(labels, ((0, 0), (0, LANES - labels.shape[1])))
    rows = jnp.concatenate([normed, labels], axis=1)
    outgoing = jnp.dot(select, rows, preferred_element_type=jnp.float32).astype(jnp.bfloat16)
    outgoing = outgoing.reshape(seq_ranks, capacity, width + LANES)
    arrived = lax.all_to_all(outgoing, "sp", split_axis=0, concat_axis=0, tiled=True)
    blocks = {0: arrived.reshape(block_rows, width + LANES)}
    bits = [1 << b for b in range(shards.bit_length() - 1)]
    for bit in reversed(bits):
        blocks.update({k | bit: flipped(v, "tp", bit) for k, v in blocks.items()})
    down = w_down.reshape(local_experts * w_down.shape[1], width)
    parts = {}
    for k, block in blocks.items():
        features = block[:, :width]
        marks = block[:, width:].astype(jnp.float32)
        hidden = []
        for expert in range(local_experts):
            gate = jnp.dot(features, w_gate[expert], preferred_element_type=jnp.float32)
            upper = jnp.dot(features, w_up[expert], preferred_element_type=jnp.float32)
            scale = marks[:, expert] + marks[:, local_experts + expert]
            hidden.append((jax.nn.silu(gate) * upper * scale[:, None]).astype(jnp.bfloat16))
        hidden = jnp.concatenate(hidden, axis=1)
        parts[k] = jnp.dot(hidden, down, preferred_element_type=jnp.float32)
    for bit in bits:
        for k in [k for k in parts if k & bit]:
            parts[k ^ bit] += flipped(parts.pop(k).astype(jnp.bfloat16), "tp", bit).astype(
                jnp.float32
            )
    summed = parts[0].astype(jnp.bfloat16).reshape(seq_ranks, capacity, width)
    returned = lax.all_to_all(summed, "sp", split_axis=0, concat_axis=0, tiled=True)
    weighted = lax.dot_general(
        select,
        returned.reshape(block_rows, width),
        (((0,), (0,)), ((), ())),
        preferred_element_type=jnp.float32,
    )
    return (stream + weighted).astype(jnp.bfloat16)


def route_by_expert(stream, normed, routes, route_weight, w_gate, w_up, w_down):
    shards = lax.axis_size("tp")
    seq_ranks = lax.axis_size("sp")
    block_rows, width = stream.shape
    local_experts = w_gate.shape[0]
    experts = local_experts * seq_ranks
    capacity = 2 * block_rows // experts
    flat_routes = routes.reshape(-1)
    position = jnp.arange(flat_routes.shape[0], dtype=jnp.int32)
    earlier = (flat_routes[:, None] == flat_routes[None, :]) & (
        position[None, :] < position[:, None]
    )
    rank = jnp.sum(earlier.astype(jnp.int32), axis=1)
    slot = flat_routes * capacity + rank
    outgoing = (
        jnp.zeros((experts * capacity, width), jnp.bfloat16).at[slot].set(normed[position // 2])
    )
    outgoing = outgoing.reshape(seq_ranks, local_experts, capacity, width)
    spread = lax.all_gather(
        lax.all_to_all(outgoing, "sp", split_axis=0, concat_axis=0, tiled=True)[:, None],
        "tp",
        axis=1,
        tiled=True,
    )
    count = spread.shape[3]
    partials = []
    for expert in range(local_experts):
        rows = spread[:, :, expert].reshape(seq_ranks * shards * count, width)
        gate = jnp.dot(rows, w_gate[expert], preferred_element_type=jnp.float32)
        upper = jnp.dot(rows, w_up[expert], preferred_element_type=jnp.float32)
        hidden = (jax.nn.silu(gate) * upper).astype(jnp.bfloat16)
        part = jnp.dot(hidden, w_down[expert], preferred_element_type=jnp.float32).astype(
            jnp.bfloat16
        )
        partials.append(part.reshape(seq_ranks, shards, count, width))
    stacked = jnp.stack(partials, axis=2)
    summed = lax.psum_scatter(stacked, "tp", scatter_dimension=1, tiled=True).astype(jnp.float32)
    returned = lax.all_to_all(
        summed[:, 0].astype(jnp.bfloat16), "sp", split_axis=0, concat_axis=0, tiled=True
    )
    results = returned.reshape(experts * capacity, width)[slot]
    results = results.reshape(block_rows, 2, width).astype(jnp.float32)
    weighted = jnp.sum(route_weight[:, :, None] * results, axis=1)
    return (stream + weighted).astype(jnp.bfloat16)


def on_device(
    conv_input,
    pre_gate,
    post_gate,
    conv_taps,
    out_proj,
    residual_in,
    norm_gain,
    routes,
    route_weight,
    w_gate,
    w_up,
    w_down,
):
    shards = lax.axis_size("tp")
    mixed = mix(conv_input, pre_gate, post_gate, conv_taps)
    stream, normed = project(mixed, out_proj, residual_in, norm_gain)
    whole_groups = lax.axis_size("sp") == GROUPS and shards & shards - 1 == 0
    route = route_by_group if whole_groups else route_by_expert
    return route(stream, normed, routes, route_weight, w_gate, w_up, w_down)


def solution(mesh):
    return jax.shard_map(
        on_device,
        mesh=mesh,
        in_specs=(
            P(("grp", "sp"), "tp"),
            P(("grp", "sp"), "tp"),
            P(("grp", "sp"), "tp"),
            P(),
            P(),
            P(("grp", "sp", "tp"), None),
            P(),
            P(("grp", "sp", "tp"), None),
            P(("grp", "sp", "tp"), None),
            P("sp", None, "tp"),
            P("sp", None, "tp"),
            P("sp", "tp", None),
        ),
        out_specs=P(("grp", "sp", "tp"), None),
        check_vma=False,
    )
```

profile of v0, /device:TPU:0, one launch (start us, length us, event | category | flops | bytes accessed | tf_op | source)
XLA Modules:
  0.0 97.2 jit_solution(9595113881826151975)
XLA Ops:
  0.0 0.8 slice.127
  0.8 0.7 slice.128
  1.5 5.0 %collective-permute-start = (bf16[2,512]{1,0:T(2,128)(2,1)S(1)}, bf16[2,512]{1,0:T(2,128)(2,1)S(1)}, u32[]{:S(2)}, u32[]{:S(2)}) collective-permute-start(bf16[2,512]{1,0:T(2,128)(2,1)S(1)} %pad_maximum_fusion.1), channel_id=1, source_target_pairs={{0,4},{4,8},{8,12},{1,5},{5,9},{9,13},{2,6},{6,10},{10,14},{3,7},{... | collective-permute-start | bytes 6152 | tf_op jit(solution)/shard_map/ppermute | solution.py:13
  6.5 0.7 fusion.111
  7.2 0.7 and_select_fusion.2
  7.9 0.7 and_select_fusion
  8.6 1.1 %convert_multiply_fusion = f32[512,256]{1,0:T(8,128)S(1)} fusion(bf16[512,256]{1,0:T(8,128)(2,1)} %param.12, bf16[512,256]{1,0:T(8,128)(2,1)} %param.13), kind=kLoop, calls=%fused_computation.78 | loop fusion | flops 393216 | bytes 1048576 | tf_op jit(solution)/shard_map/mul | solution.py:29
  9.7 0.7 fusion.108
  10.6 0.9 fusion.119
  11.6 1.9 %fusion.62 = bf16[512,256]{1,0:T(8,128)(2,1)} fusion(f32[2,256]{1,0:T(2,128)S(1)} %convert_multiply_fusion.1, f32[512,256]{1,0:T(8,128)S(1)} %convert_multiply_fusion, bf16[512,256]{1,0:T(8,128)(2,1)} %param.14, f32[256]{0:T(256)S(1)} %bitcast.96, f32[256]{0:T(256)S(1)} %bitcast.95, f32[256]{0:T(256)S(1)} %bitcast.94), kind=kLoop, calls=%fused_computation.75 | loop fusion | flops 1310720 | bytes 1053696 | tf_op jit(solution)/shard_map/convert_element_type | solution.py:34
  13.5 3.4 %all-to-all-start = ((bf16[4,128,256]{2,1,0:T(8,128)(2,1)}), bf16[4,128,256]{2,1,0:T(8,128)(2,1)S(1)}, u32[]{:S(2)}, u32[]{:S(2)}) async-start(bf16[4,128,256]{2,1,0:T(8,128)(2,1)} %bitcast.3), calls=%async_computation | async-start | bytes 524288 | tf_op jit(solution)/shard_map/all_to_all | solution.py:38
  16.9 5.9 %all-to-all-done = bf16[4,128,256]{2,1,0:T(8,128)(2,1)S(1)} async-done(((bf16[4,128,256]{2,1,0:T(8,128)(2,1)}), bf16[4,128,256]{2,1,0:T(8,128)(2,1)S(1)}, u32[]{:S(2)}, u32[]{:S(2)}) %all-to-all-start) | async-done | bytes 262176 | tf_op jit(solution)/shard_map/all_to_all | solution.py:38
  23.0 3.0 %multiply_reduce_fusion = (f32[128]{0:T(128)S(1)}, f32[128,2048]{1,0:T(8,128)S(1)}) fusion(bf16[128,1024]{0,1:T(8,128)(2,1)S(1)} %bitcast.84, bf16[1024,2048]{1,0:T(8,128)(2,1)} %param.16, bf16[128,2048]{1,0:T(8,128)(2,1)S(1)} %copy-done.1), kind=kOutput, calls=%fused_computation.47 | convolution fusion | flops 537919360 | bytes 6029824 | tf_op jit(solution)/shard_map/dot_general | solution.py:39
  26.6 18.7 %all_to_all.29 = bf16[4,32,2176]{2,1,0:T(8,128)(2,1)S(1)} all-to-all(bf16[4,32,2176]{2,1,0:T(8,128)(2,1)S(1)} %bitcast.93), channel_id=1, replica_groups=mesh['grp'=2,'sp'=4,'tp'=4] {'sp'}, dimensions={0} | all-to-all | bytes 1114112 | tf_op jit(solution)/shard_map/all_to_all | solution.py:65
  45.3 0.8 collective-permute-start.3
  47.3 0.8 collective-permute-done.1
  50.0 8.4 %collective-permute-done.3 = bf16[128,2176]{1,0:T(8,128)(2,1)S(1)} collective-permute-done((bf16[128,2176]{1,0:T(8,128)(2,1)S(1)}, bf16[128,2176]{1,0:T(8,128)(2,1)S(1)}, u32[]{:S(2)}, u32[]{:S(2)}) %collective-permute-start.3) | collective-permute-done | bytes 557088 | tf_op jit(solution)/shard_map/ppermute | solution.py:17
  58.6 0.6 collective-permute-start.2
  59.9 0.5 collective-permute-done.4
  63.2 1.1 %collective-permute-done.5 = bf16[128,2048]{1,0:T(8,128)(2,1)S(1)} collective-permute-done((bf16[128,2048]{1,0:T(8,128)(2,1)S(1)}, bf16[128,2048]{1,0:T(8,128)(2,1)S(1)}, u32[]{:S(2)}, u32[]{:S(2)}) %collective-permute-start.5) | collective-permute-done | bytes 524320 | tf_op jit(solution)/shard_map/ppermute | solution.py:17
  64.8 1.4 %collective-permute-start.6 = (bf16[128,2048]{1,0:T(8,128)(2,1)S(1)}, bf16[128,2048]{1,0:T(8,128)(2,1)S(1)}, u32[]{:S(2)}, u32[]{:S(2)}) collective-permute-start(bf16[128,2048]{1,0:T(8,128)(2,1)S(1)} %add_convert_fusion.1), channel_id=1, source_target_pairs={{0,2},{1,3},{2,0},{3,1},{4,6},{5,7},{6,4},{7,5},{8,10},{9,11},{10,... | collective-permute-start | bytes 1572872 | tf_op jit(solution)/shard_map/ppermute | solution.py:17
  67.0 11.9 %collective-permute-done.6 = bf16[128,2048]{1,0:T(8,128)(2,1)S(1)} collective-permute-done((bf16[128,2048]{1,0:T(8,128)(2,1)S(1)}, bf16[128,2048]{1,0:T(8,128)(2,1)S(1)}, u32[]{:S(2)}, u32[]{:S(2)}) %collective-permute-start.6) | collective-permute-done | bytes 524320 | tf_op jit(solution)/shard_map/ppermute | solution.py:17
  79.0 17.0 %all_to_all.30 = bf16[4,32,2048]{2,1,0:T(8,128)(2,1)S(1)} all-to-all(bf16[4,32,2048]{2,1,0:T(8,128)(2,1)S(1)} %bitcast.82), channel_id=1, replica_groups=mesh['grp'=2,'sp'=4,'tp'=4] {'sp'}, dimensions={0} | all-to-all | bytes 1048576 | tf_op jit(solution)/shard_map/all_to_all | solution.py:89
  96.1 1.1 %fusion = bf16[128,2048]{1,0:T(8,128)(2,1)} fusion(f32[128,2048]{1,0:T(8,128)S(1)} %get-tuple-element.19, bf16[128,2048]{1,0:T(8,128)(2,1)S(1)} %bitcast.83, s32[128]{0:T(128)S(1)} %multiply_add_fusion), kind=kOutput, calls=%fused_computation.3 | convolution fusion | flops 67649536 | bytes 2097664 | tf_op jit(solution)/shard_map/dot_general | solution.py:90
  (57 shorter events, 9.2 us)
Async XLA Ops:
  0.0 49.6 %copy-start = (bf16[2,256,2048]{2,1,0:T(8,128)(2,1)S(1)}, bf16[2,256,2048]{2,1,0:T(8,128)(2,1)}, u32[]{:S(2)}) copy-start(bf16[2,256,2048]{2,1,0:T(8,128)(2,1)} %param.23) | copy-start | bytes 6291460
  0.0 16.9 %copy-start.3 = (s32[128,2]{0,1:T(2,128)S(1)}, s32[128,2]{0,1:T(2,128)}, u32[]{:S(2)}) copy-start(s32[128,2]{0,1:T(2,128)} %param.19) | copy-start | bytes 3076
  0.0 23.0 %copy-start.1 = (bf16[128,2048]{1,0:T(8,128)(2,1)S(1)}, bf16[128,2048]{1,0:T(8,128)(2,1)}, u32[]{:S(2)}) copy-start(bf16[128,2048]{1,0:T(8,128)(2,1)} %param.17) | copy-start | bytes 1572868
  1.5 10.0 %collective-permute-start = (bf16[2,512]{1,0:T(2,128)(2,1)S(1)}, bf16[2,512]{1,0:T(2,128)(2,1)S(1)}, u32[]{:S(2)}, u32[]{:S(2)}) collective-permute-start(bf16[2,512]{1,0:T(2,128)(2,1)S(1)} %pad_maximum_fusion.1), channel_id=1, source_target_pairs={{0,4},{4,8},{8,12},{1,5},{5,9},{9,13},{2,6},{6,10},{10,14},{3,7},{... | collective-permute-start | bytes 6152 | tf_op jit(solution)/shard_map/ppermute | solution.py:13
  13.5 9.4 %all-to-all-start = ((bf16[4,128,256]{2,1,0:T(8,128)(2,1)}), bf16[4,128,256]{2,1,0:T(8,128)(2,1)S(1)}, u32[]{:S(2)}, u32[]{:S(2)}) async-start(bf16[4,128,256]{2,1,0:T(8,128)(2,1)} %bitcast.3), calls=%async_computation | async-start | bytes 524288 | tf_op jit(solution)/shard_map/all_to_all | solution.py:38
  23.0 3.0 %copy-start.2 = (f32[2048]{0:T(1024)S(1)}, f32[2048]{0:T(1024)}, u32[]{:S(2)}) copy-start(f32[2048]{0:T(1024)} %param.18) | copy-start | bytes 24580
  26.1 20.0 %copy-start.4 = (bf16[2,2048,256]{2,1,0:T(8,128)(2,1)S(1)}, bf16[2,2048,256]{2,1,0:T(8,128)(2,1)}, u32[]{:S(2)}) copy-start(bf16[2,2048,256]{2,1,0:T(8,128)(2,1)} %param.21) | copy-start | bytes 6291460
  45.3 1.7 %copy-start.5 = (bf16[2,2048,256]{2,1,0:T(8,128)(2,1)S(1)}, bf16[2,2048,256]{2,1,0:T(8,128)(2,1)}, u32[]{:S(2)}) copy-start(bf16[2,2048,256]{2,1,0:T(8,128)(2,1)} %param.22) | copy-start | bytes 6291460
  45.3 13.2 %collective-permute-start.3 = (bf16[128,2176]{1,0:T(8,128)(2,1)S(1)}, bf16[128,2176]{1,0:T(8,128)(2,1)S(1)}, u32[]{:S(2)}, u32[]{:S(2)}) collective-permute-start(bf16[128,2176]{1,0:T(8,128)(2,1)S(1)} %bitcast.87), channel_id=1, source_target_pairs={{0,2},{1,3},{2,0},{3,1},{4,6},{5,7},{6,4},{7,5},{8,10},{9,11},{10,... | collective-permute-start | bytes 1671176 | tf_op jit(solution)/shard_map/ppermute | solution.py:17
  46.1 2.0 %collective-permute-start.1 = (bf16[128,2176]{1,0:T(8,128)(2,1)S(1)}, bf16[128,2176]{1,0:T(8,128)(2,1)S(1)}, u32[]{:S(2)}, u32[]{:S(2)}) collective-permute-start(bf16[128,2176]{1,0:T(8,128)(2,1)S(1)} %bitcast.88), channel_id=1, source_target_pairs={{0,1},{1,0},{2,3},{3,2},{4,5},{5,4},{6,7},{7,6},{8,9},{9,8},{10,11... | collective-permute-start | bytes 1671176 | tf_op jit(solution)/shard_map/ppermute | solution.py:17
  58.4 2.0 %collective-permute-start.4 = (bf16[128,2176]{1,0:T(8,128)(2,1)S(1)}, bf16[128,2176]{1,0:T(8,128)(2,1)S(1)}, u32[]{:S(2)}, u32[]{:S(2)}) collective-permute-start(bf16[128,2176]{1,0:T(8,128)(2,1)S(1)} %collective-permute-done.3), channel_id=1, source_target_pairs={{0,1},{1,0},{2,3},{3,2},{4,5},{5,4},{6,7},{7,6},{8,9},{9,8},{10,11... | collective-permute-start | bytes 1671176 | tf_op jit(solution)/shard_map/ppermute | solution.py:17
  58.6 8.3 %collective-permute-start.2 = (bf16[128,2048]{1,0:T(8,128)(2,1)S(1)}, bf16[128,2048]{1,0:T(8,128)(2,1)S(1)}, u32[]{:S(2)}, u32[]{:S(2)}) collective-permute-start(bf16[128,2048]{1,0:T(8,128)(2,1)S(1)} %convolution_convert_fusion.2), channel_id=1, source_target_pairs={{0,1},{1,0},{2,3},{3,2},{4,5},{5,4},{6,7},{7,6},{8,9},{9,8},{10,11... | collective-permute-start | bytes 1572872 | tf_op jit(solution)/shard_map/ppermute | solution.py:17
  62.4 2.0 %collective-permute-start.5 = (bf16[128,2048]{1,0:T(8,128)(2,1)S(1)}, bf16[128,2048]{1,0:T(8,128)(2,1)S(1)}, u32[]{:S(2)}, u32[]{:S(2)}) collective-permute-start(bf16[128,2048]{1,0:T(8,128)(2,1)S(1)} %convolution_convert_fusion.1), channel_id=1, source_target_pairs={{0,1},{1,0},{2,3},{3,2},{4,5},{5,4},{6,7},{7,6},{8,9},{9,8},{10,11... | collective-permute-start | bytes 1572872 | tf_op jit(solution)/shard_map/ppermute | solution.py:17
  64.8 14.0 %collective-permute-start.6 = (bf16[128,2048]{1,0:T(8,128)(2,1)S(1)}, bf16[128,2048]{1,0:T(8,128)(2,1)S(1)}, u32[]{:S(2)}, u32[]{:S(2)}) collective-permute-start(bf16[128,2048]{1,0:T(8,128)(2,1)S(1)} %add_convert_fusion.1), channel_id=1, source_target_pairs={{0,2},{1,3},{2,0},{3,1},{4,6},{5,7},{6,4},{7,5},{8,10},{9,11},{10,... | collective-permute-start | bytes 1572872 | tf_op jit(solution)/shard_map/ppermute | solution.py:17
where the time goes:
time: 97.7 us; the launch traced here: 97.2 us
  blocking collectives  35.7 us (37%)
  waiting for transfers between devices  28.6 us (29%)
  matrix products  11.4 us (12%)
  starting transfers between devices  11.3 us (12%)
  other arithmetic  7.07 us (7%)
  local copies, waits for them, and re-layouts  2.75 us (3%)
    ppermute x6, waiting for transfers between devices, flipped(): lax.ppermute(block, axis, [(i, i ^ bit) for i in range(lax.axis_size(axis...  22.7 us
    all_to_all x1, blocking collectives, route_by_group(): lax.all_to_all(outgoing, 'sp', split_axis=0, concat_axis=0, tiled=True)  18.7 us
    all_to_all x1, blocking collectives, route_by_group(): lax.all_to_all(summed, 'sp', split_axis=0, concat_axis=0, tiled=True)  17 us
    all_to_all x1, waiting for transfers between devices, project(): lax.all_to_all(mixed, 'tp', split_axis=0, concat_axis=1, tiled=True)  5.94 us
    ppermute x1, starting transfers between devices, shifted(): return lax.ppermute(block, axis, route)  4.96 us
    all_to_all x1, starting transfers between devices, project(): lax.all_to_all(mixed, 'tp', split_axis=0, concat_axis=1, tiled=True)  3.41 us
    dot_general x1, matrix products, project(): jnp.dot(token_rows, out_proj, preferred_element_type=jnp.float32)  3.01 us
    ppermute x6, starting transfers between devices, flipped(): lax.ppermute(block, axis, [(i, i ^ bit) for i in range(lax.axis_size(axis...  2.97 us
  transfers between devices with their start and end apart: 8, of which 6 were waited for; matrix products, arithmetic and copies ran while one was open for 13% of the time, Pallas kernels for 0%

commit v1 on v0

--- a/solution.py
+++ b/solution.py
@@ -5,6 +5,29 @@
 
 GROUPS = 4
 LANES = 128
+
+
+def split_up(x, dim, length):
+    dims = x.shape
+    blocks = x.reshape(*dims[:dim], length, dims[dim] // length, *dims[dim + 1 :])
+    return jnp.moveaxis(blocks, dim, 0)
+
+
+def joined_along(blocks, dim):
+    blocks = jnp.moveaxis(blocks, 0, dim)
+    dims = blocks.shape
+    return blocks.reshape(*dims[:dim], dims[dim] * dims[dim + 1], *dims[dim + 2 :])
+
+
+def exchange_directly(x, axis, split_dim, concat_dim):
+    devices, index = (lax.axis_size(axis), lax.axis_index(axis))
+    tiles = split_up(x, split_dim, devices)
+    done = [tiles[index]]
+    for lap in range(1, devices):
+        sent = tiles[(index + lap) % devices]
+        done.append(lax.ppermute(sent, axis, [(i, (i + lap) % devices) for i in range(devices)]))
+    tiles = jnp.stack(done)[(index - jnp.arange(devices)) % devices]
+    return joined_along(tiles, concat_dim)
 
 
 def shifted(block, axis, distance):
@@ -62,7 +85,7 @@
     rows = jnp.concatenate([normed, labels], axis=1)
     outgoing = jnp.dot(select, rows, preferred_element_type=jnp.float32).astype(jnp.bfloat16)
     outgoing = outgoing.reshape(seq_ranks, capacity, width + LANES)
-    arrived = lax.all_to_all(outgoing, "sp", split_axis=0, concat_axis=0, tiled=True)
+    arrived = exchange_directly(outgoing, "sp", 0, 0)
     blocks = {0: arrived.reshape(block_rows, width + LANES)}
     bits = [1 << b for b in range(shards.bit_length() - 1)]
     for bit in reversed(bits):

time: 97.7 us -> 99.3 us (1.016)
  blocking collectives: 35.7 us -> 17.6 us
  waiting for transfers between devices: 28.6 us -> 36.9 us
  starting transfers between devices: 11.3 us -> 15.8 us
  matrix products: 11.4 us -> 14.1 us
  local copies, waits for them, and re-layouts: 2.75 us -> 5.26 us
  other arithmetic: 7.07 us -> 8.78 us
    all_to_all x1 -> x0, blocking collectives: 18.7 us -> none  [route_by_group(): lax.all_to_all(outgoing, 'sp', split_axis=0, concat_axis=0, tiled=True)]
    ppermute x0 -> x3, waiting for transfers between devices: none -> 10.4 us  [exchange_directly(): lax.ppermute(sent, axis, [(i, (i + lap) % devices) for i in range(devices)])]
    ppermute x0 -> x3, starting transfers between devices: none -> 4.67 us  [exchange_directly(): lax.ppermute(sent, axis, [(i, (i + lap) % devices) for i in range(devices)])]
    dot_general x8, matrix products: 2.56 us -> 5.22 us  [route_by_group(): gate = jnp.dot(features, w_gate[expert], preferred_element_type=jnp.float32)]
    gather x0 -> x1, local copies, waits for them, and re-layouts: none -> 2.45 us  [exchange_directly(): tiles = jnp.stack(done)[(index - jnp.arange(devices)) % devices]]
    ppermute x6, waiting for transfers between devices: 22.7 us -> 20.5 us  [flipped(): lax.ppermute(block, axis, [(i, i ^ bit) for i in range(lax.axis_size(axis...]
  transfers between devices with their start and end apart: 8 -> 11, of which waited for: 6 -> 7; matrix products, arithmetic and copies ran while one was open for 13% -> 16% of each run, Pallas kernels for 0% -> 0%
where the time goes in v1:
time: 99.3 us; the launch traced here: 98.8 us
  waiting for transfers between devices  36.9 us (37%)
  blocking collectives  17.6 us (18%)
  starting transfers between devices  15.8 us (16%)
  matrix products  14.1 us (14%)
  other arithmetic  8.78 us (9%)
  local copies, waits for them, and re-layouts  5.26 us (5%)
    ppermute x6, waiting for transfers between devices, flipped(): lax.ppermute(block, axis, [(i, i ^ bit) for i in range(lax.axis_size(axis...  20.5 us
    all_to_all x1, blocking collectives, route_by_group(): lax.all_to_all(summed, 'sp', split_axis=0, concat_axis=0, tiled=True)  17.6 us
    ppermute x3, waiting for transfers between devices, exchange_directly(): lax.ppermute(sent, axis, [(i, (i + lap) % devices) for i in range(devices)])  10.4 us
    all_to_all x1, waiting for transfers between devices, project(): lax.all_to_all(mixed, 'tp', split_axis=0, concat_axis=1, tiled=True)  5.94 us
    dot_general x8, matrix products, route_by_group(): gate = jnp.dot(features, w_gate[expert], preferred_element_type=jnp.float32)  5.22 us
    ppermute x1, starting transfers between devices, shifted(): return lax.ppermute(block, axis, route)  4.95 us
    ppermute x3, starting transfers between devices, exchange_directly(): lax.ppermute(sent, axis, [(i, (i + lap) % devices) for i in range(devices)])  4.67 us
    all_to_all x1, starting transfers between devices, project(): lax.all_to_all(mixed, 'tp', split_axis=0, concat_axis=1, tiled=True)  3.41 us
  transfers between devices with their start and end apart: 11, of which 7 were waited for; matrix products, arithmetic and copies ran while one was open for 16% of the time, Pallas kernels for 0%

profile of v1, /device:TPU:0, one launch (start us, length us, event | category | flops | bytes accessed | tf_op | source)
XLA Modules:
  0.0 98.8 jit_solution(16989813809686866853)
XLA Ops:
  0.0 0.9 slice.127
  1.6 5.0 %collective-permute-start = (bf16[2,512]{1,0:T(2,128)(2,1)S(1)}, bf16[2,512]{1,0:T(2,128)(2,1)S(1)}, u32[]{:S(2)}, u32[]{:S(2)}) collective-permute-start(bf16[2,512]{1,0:T(2,128)(2,1)S(1)} %pad_maximum_fusion.1), channel_id=1, source_target_pairs={{0,4},{4,8},{8,12},{1,5},{5,9},{9,13},{2,6},{6,10},{10,14},{3,7},{... | collective-permute-start | bytes 6152 | tf_op jit(solution)/shard_map/ppermute | solution.py:36
  8.6 1.1 %convert_multiply_fusion = f32[512,256]{1,0:T(8,128)S(1)} fusion(bf16[512,256]{1,0:T(8,128)(2,1)} %param.12, bf16[512,256]{1,0:T(8,128)(2,1)} %param.13), kind=kLoop, calls=%fused_computation.80 | loop fusion | flops 393216 | bytes 1048576 | tf_op jit(solution)/shard_map/mul | solution.py:52
  10.6 0.9 fusion.121
  11.6 1.9 %fusion.62 = bf16[512,256]{1,0:T(8,128)(2,1)} fusion(f32[2,256]{1,0:T(2,128)S(1)} %convert_multiply_fusion.1, f32[512,256]{1,0:T(8,128)S(1)} %convert_multiply_fusion, bf16[512,256]{1,0:T(8,128)(2,1)} %param.14, f32[256]{0:T(256)S(1)} %bitcast.112, f32[256]{0:T(256)S(1)} %bitcast.111, f32[256]{0:T(256)S(1)} %bitcast.110), kind=kLoop, calls=%fused_computation.77 | loop fusion | flops 1310720 | bytes 1053696 | tf_op jit(solution)/shard_map/convert_element_type | solution.py:57
  13.5 3.4 %all-to-all-start = ((bf16[4,128,256]{2,1,0:T(8,128)(2,1)}), bf16[4,128,256]{2,1,0:T(8,128)(2,1)S(1)}, u32[]{:S(2)}, u32[]{:S(2)}) async-start(bf16[4,128,256]{2,1,0:T(8,128)(2,1)} %bitcast.3), calls=%async_computation | async-start | bytes 524288 | tf_op jit(solution)/shard_map/all_to_all | solution.py:61
  16.9 5.9 %all-to-all-done = bf16[4,128,256]{2,1,0:T(8,128)(2,1)S(1)} async-done(((bf16[4,128,256]{2,1,0:T(8,128)(2,1)}), bf16[4,128,256]{2,1,0:T(8,128)(2,1)S(1)}, u32[]{:S(2)}, u32[]{:S(2)}) %all-to-all-start) | async-done | bytes 262176 | tf_op jit(solution)/shard_map/all_to_all | solution.py:61
  23.1 3.1 %multiply_reduce_fusion = (f32[128]{0:T(128)S(1)}, f32[128,2048]{1,0:T(8,128)S(1)}) fusion(bf16[128,1024]{0,1:T(8,128)(2,1)S(1)} %bitcast.97, bf16[1024,2048]{1,0:T(8,128)(2,1)} %param.16, bf16[128,2048]{1,0:T(8,128)(2,1)} %param.17), kind=kOutput, calls=%fused_computation.48 | convolution fusion | flops 537919360 | bytes 6029824 | tf_op jit(solution)/shard_map/dot_general | solution.py:62
  26.7 1.5 %collective-permute-start.3 = (bf16[1,32,2176]{2,1,0:T(8,128)(2,1)S(1)}, bf16[1,32,2176]{2,1,0:T(8,128)(2,1)S(1)}, u32[]{:S(2)}, u32[]{:S(2)}) collective-permute-start(bf16[1,32,2176]{2,1,0:T(8,128)(2,1)S(1)} %get-tuple-element.14), channel_id=1, source_target_pairs={{0,12},{4,0},{8,4},{12,8},{1,13},{5,1},{9,5},{13,9},{2,14},{6,2},{... | collective-permute-start | bytes 417800 | tf_op jit(solution)/shard_map/ppermute | solution.py:28
  28.2 1.6 %collective-permute-start.2 = (bf16[1,32,2176]{2,1,0:T(8,128)(2,1)S(1)}, bf16[1,32,2176]{2,1,0:T(8,128)(2,1)S(1)}, u32[]{:S(2)}, u32[]{:S(2)}) collective-permute-start(bf16[1,32,2176]{2,1,0:T(8,128)(2,1)S(1)} %get-tuple-element.15), channel_id=1, source_target_pairs={{0,8},{4,12},{8,0},{12,4},{1,9},{5,13},{9,1},{13,5},{2,10},{6,14},... | collective-permute-start | bytes 417800 | tf_op jit(solution)/shard_map/ppermute | solution.py:28
  29.8 1.6 %collective-permute-start.1 = (bf16[1,32,2176]{2,1,0:T(8,128)(2,1)S(1)}, bf16[1,32,2176]{2,1,0:T(8,128)(2,1)S(1)}, u32[]{:S(2)}, u32[]{:S(2)}) collective-permute-start(bf16[1,32,2176]{2,1,0:T(8,128)(2,1)S(1)} %get-tuple-element.16), channel_id=1, source_target_pairs={{0,4},{4,8},{8,12},{12,0},{1,5},{5,9},{9,13},{13,1},{2,6},{6,10},{... | collective-permute-start | bytes 417800 | tf_op jit(solution)/shard_map/ppermute | solution.py:28
  31.4 0.9 collective-permute-done.3
  32.3 9.6 %collective-permute-done.2 = bf16[1,32,2176]{2,1,0:T(8,128)(2,1)S(1)} collective-permute-done((bf16[1,32,2176]{2,1,0:T(8,128)(2,1)S(1)}, bf16[1,32,2176]{2,1,0:T(8,128)(2,1)S(1)}, u32[]{:S(2)}, u32[]{:S(2)}) %collective-permute-start.2) | collective-permute-done | bytes 139296 | tf_op jit(solution)/shard_map/ppermute | solution.py:28
  41.9 0.9 maximum_bitcast_fusion
  42.8 2.5 %gather_fusion = bf16[4,32,2176]{2,1,0:T(8,128)(2,1)} fusion(bf16[4,32,2176]{2,1,0:T(8,128)(2,1)} %maximum_bitcast_fusion, s32[1024]{0:T(1024)S(1)} %pad_clamp_fusion), kind=kCustom, calls=%fused_computation | custom fusion | bytes 1114128 | tf_op jit(solution)/shard_map/gather | solution.py:29
  45.2 0.8 slice_convert_fusion.3
  46.8 1.7 %fusion.19 = f32[128,256]{1,0:T(8,128)S(1)} fusion(bf16[2,2048,256]{2,1,0:T(8,128)(2,1)} %param.21, bf16[128,2176]{1,0:T(8,128)(2,1)} %bitcast.102), kind=kOutput, calls=%fused_computation.28 | convolution fusion | flops 134217728 | bytes 1703936 | tf_op jit(solution)/shard_map/dot_general | solution.py:100
  48.7 1.7 %fusion.34 = f32[128,256]{1,0:T(8,128)S(1)} fusion(bf16[2,2048,256]{2,1,0:T(8,128)(2,1)} %param.21, bf16[128,2176]{1,0:T(8,128)(2,1)S(1)} %bitcast.103), kind=kOutput, calls=%fused_computation.43 | convolution fusion | flops 134217728 | bytes 1703936 | tf_op jit(solution)/shard_map/dot_general | solution.py:100
  52.7 6.8 %collective-permute-done.6 = bf16[128,2176]{1,0:T(8,128)(2,1)S(1)} collective-permute-done((bf16[128,2176]{1,0:T(8,128)(2,1)}, bf16[128,2176]{1,0:T(8,128)(2,1)S(1)}, u32[]{:S(2)}, u32[]{:S(2)}) %collective-permute-start.6) | collective-permute-done | bytes 557088 | tf_op jit(solution)/shard_map/ppermute | solution.py:40
  64.2 1.1 %collective-permute-done.8 = bf16[128,2048]{1,0:T(8,128)(2,1)S(1)} collective-permute-done((bf16[128,2048]{1,0:T(8,128)(2,1)S(1)}, bf16[128,2048]{1,0:T(8,128)(2,1)S(1)}, u32[]{:S(2)}, u32[]{:S(2)}) %collective-permute-start.8) | collective-permute-done | bytes 524320 | tf_op jit(solution)/shard_map/ppermute | solution.py:40
  65.8 1.2 %collective-permute-start.9 = (bf16[128,2048]{1,0:T(8,128)(2,1)S(1)}, bf16[128,2048]{1,0:T(8,128)(2,1)S(1)}, u32[]{:S(2)}, u32[]{:S(2)}) collective-permute-start(bf16[128,2048]{1,0:T(8,128)(2,1)S(1)} %add_convert_fusion.1), channel_id=1, source_target_pairs={{0,2},{1,3},{2,0},{3,1},{4,6},{5,7},{6,4},{7,5},{8,10},{9,11},{10,... | collective-permute-start | bytes 1572872 | tf_op jit(solution)/shard_map/ppermute | solution.py:40
  67.8 12.1 %collective-permute-done.9 = bf16[128,2048]{1,0:T(8,128)(2,1)S(1)} collective-permute-done((bf16[128,2048]{1,0:T(8,128)(2,1)S(1)}, bf16[128,2048]{1,0:T(8,128)(2,1)S(1)}, u32[]{:S(2)}, u32[]{:S(2)}) %collective-permute-start.9) | collective-permute-done | bytes 524320 | tf_op jit(solution)/shard_map/ppermute | solution.py:40
  80.0 17.6 %all_to_all.24 = bf16[4,32,2048]{2,1,0:T(8,128)(2,1)S(1)} all-to-all(bf16[4,32,2048]{2,1,0:T(8,128)(2,1)S(1)} %bitcast.95), channel_id=1, replica_groups=mesh['grp'=2,'sp'=4,'tp'=4] {'sp'}, dimensions={0} | all-to-all | bytes 1048576 | tf_op jit(solution)/shard_map/all_to_all | solution.py:112
  97.7 1.1 %fusion = bf16[128,2048]{1,0:T(8,128)(2,1)} fusion(f32[128,2048]{1,0:T(8,128)S(1)} %get-tuple-element.23, bf16[128,2048]{1,0:T(8,128)(2,1)S(1)} %bitcast.96, s32[128]{0:T(128)S(1)} %multiply_add_fusion), kind=kOutput, calls=%fused_computation.4 | convolution fusion | flops 67649536 | bytes 2097664 | tf_op jit(solution)/shard_map/dot_general | solution.py:113
  (67 shorter events, 13.7 us)
Async XLA Ops:
  0.0 52.2 %copy-start = (bf16[2,256,2048]{2,1,0:T(8,128)(2,1)S(1)}, bf16[2,256,2048]{2,1,0:T(8,128)(2,1)}, u32[]{:S(2)}) copy-start(bf16[2,256,2048]{2,1,0:T(8,128)(2,1)} %param.23) | copy-start | bytes 6291460
  0.0 16.9 %copy-start.3 = (s32[128,2]{0,1:T(2,128)S(1)}, s32[128,2]{0,1:T(2,128)}, u32[]{:S(2)}) copy-start(s32[128,2]{0,1:T(2,128)} %param.19) | copy-start | bytes 3076
  1.6 10.0 %collective-permute-start = (bf16[2,512]{1,0:T(2,128)(2,1)S(1)}, bf16[2,512]{1,0:T(2,128)(2,1)S(1)}, u32[]{:S(2)}, u32[]{:S(2)}) collective-permute-start(bf16[2,512]{1,0:T(2,128)(2,1)S(1)} %pad_maximum_fusion.1), channel_id=1, source_target_pairs={{0,4},{4,8},{8,12},{1,5},{5,9},{9,13},{2,6},{6,10},{10,14},{3,7},{... | collective-permute-start | bytes 6152 | tf_op jit(solution)/shard_map/ppermute | solution.py:36
  13.5 9.4 %all-to-all-start = ((bf16[4,128,256]{2,1,0:T(8,128)(2,1)}), bf16[4,128,256]{2,1,0:T(8,128)(2,1)S(1)}, u32[]{:S(2)}, u32[]{:S(2)}) async-start(bf16[4,128,256]{2,1,0:T(8,128)(2,1)} %bitcast.3), calls=%async_computation | async-start | bytes 524288 | tf_op jit(solution)/shard_map/all_to_all | solution.py:61
  23.0 3.2 %copy-start.2 = (f32[2048]{0:T(1024)S(1)}, f32[2048]{0:T(1024)}, u32[]{:S(2)}) copy-start(f32[2048]{0:T(1024)} %param.18) | copy-start | bytes 24580
  26.7 5.6 %collective-permute-start.3 = (bf16[1,32,2176]{2,1,0:T(8,128)(2,1)S(1)}, bf16[1,32,2176]{2,1,0:T(8,128)(2,1)S(1)}, u32[]{:S(2)}, u32[]{:S(2)}) collective-permute-start(bf16[1,32,2176]{2,1,0:T(8,128)(2,1)S(1)} %get-tuple-element.14), channel_id=1, source_target_pairs={{0,12},{4,0},{8,4},{12,8},{1,13},{5,1},{9,5},{13,9},{2,14},{6,2},{... | collective-permute-start | bytes 417800 | tf_op jit(solution)/shard_map/ppermute | solution.py:28
  28.2 13.7 %collective-permute-start.2 = (bf16[1,32,2176]{2,1,0:T(8,128)(2,1)S(1)}, bf16[1,32,2176]{2,1,0:T(8,128)(2,1)S(1)}, u32[]{:S(2)}, u32[]{:S(2)}) collective-permute-start(bf16[1,32,2176]{2,1,0:T(8,128)(2,1)S(1)} %get-tuple-element.15), channel_id=1, source_target_pairs={{0,8},{4,12},{8,0},{12,4},{1,9},{5,13},{9,1},{13,5},{2,10},{6,14},... | collective-permute-start | bytes 417800 | tf_op jit(solution)/shard_map/ppermute | solution.py:28
  29.8 12.0 %collective-permute-start.1 = (bf16[1,32,2176]{2,1,0:T(8,128)(2,1)S(1)}, bf16[1,32,2176]{2,1,0:T(8,128)(2,1)S(1)}, u32[]{:S(2)}, u32[]{:S(2)}) collective-permute-start(bf16[1,32,2176]{2,1,0:T(8,128)(2,1)S(1)} %get-tuple-element.16), channel_id=1, source_target_pairs={{0,4},{4,8},{8,12},{12,0},{1,5},{5,9},{9,13},{13,1},{2,6},{6,10},{... | collective-permute-start | bytes 417800 | tf_op jit(solution)/shard_map/ppermute | solution.py:28
  45.2 3.5 %copy-start.1 = (bf16[4,32,2176]{2,1,0:T(8,128)(2,1)S(1)}, bf16[4,32,2176]{2,1,0:T(8,128)(2,1)}, u32[]{:S(2)}) copy-start(bf16[4,32,2176]{2,1,0:T(8,128)(2,1)} %gather_fusion) | copy-start | bytes 1671172
  46.1 4.4 %copy-start.5 = (bf16[2,2048,256]{2,1,0:T(8,128)(2,1)S(1)}, bf16[2,2048,256]{2,1,0:T(8,128)(2,1)}, u32[]{:S(2)}) copy-start(bf16[2,2048,256]{2,1,0:T(8,128)(2,1)} %param.22) | copy-start | bytes 6291460
  46.1 13.4 %collective-permute-start.6 = (bf16[128,2176]{1,0:T(8,128)(2,1)}, bf16[128,2176]{1,0:T(8,128)(2,1)S(1)}, u32[]{:S(2)}, u32[]{:S(2)}) collective-permute-start(bf16[128,2176]{1,0:T(8,128)(2,1)} %bitcast.100), channel_id=1, source_target_pairs={{0,2},{1,3},{2,0},{3,1},{4,6},{5,7},{6,4},{7,5},{8,10},{9,11},{10,... | collective-permute-start | bytes 1671176 | tf_op jit(solution)/shard_map/ppermute | solution.py:40
  46.8 3.9 %collective-permute-start.4 = (bf16[128,2176]{1,0:T(8,128)(2,1)}, bf16[128,2176]{1,0:T(8,128)(2,1)S(1)}, u32[]{:S(2)}, u32[]{:S(2)}) collective-permute-start(bf16[128,2176]{1,0:T(8,128)(2,1)} %bitcast.101), channel_id=1, source_target_pairs={{0,1},{1,0},{2,3},{3,2},{4,5},{5,4},{6,7},{7,6},{8,9},{9,8},{10,11... | collective-permute-start | bytes 1671176 | tf_op jit(solution)/shard_map/ppermute | solution.py:40
  48.7 2.3 %copy-start.4 = (bf16[2,2048,256]{2,1,0:T(8,128)(2,1)S(1)}, bf16[2,2048,256]{2,1,0:T(8,128)(2,1)}, u32[]{:S(2)}) copy-start(bf16[2,2048,256]{2,1,0:T(8,128)(2,1)} %param.21) | copy-start | bytes 6291460
  59.5 2.0 %collective-permute-start.7 = (bf16[128,2176]{1,0:T(8,128)(2,1)S(1)}, bf16[128,2176]{1,0:T(8,128)(2,1)S(1)}, u32[]{:S(2)}, u32[]{:S(2)}) collective-permute-start(bf16[128,2176]{1,0:T(8,128)(2,1)S(1)} %collective-permute-done.6), channel_id=1, source_target_pairs={{0,1},{1,0},{2,3},{3,2},{4,5},{5,4},{6,7},{7,6},{8,9},{9,8},{10,11... | collective-permute-start | bytes 1671176 | tf_op jit(solution)/shard_map/ppermute | solution.py:40
  59.7 8.1 %collective-permute-start.5 = (bf16[128,2048]{1,0:T(8,128)(2,1)S(1)}, bf16[128,2048]{1,0:T(8,128)(2,1)S(1)}, u32[]{:S(2)}, u32[]{:S(2)}) collective-permute-start(bf16[128,2048]{1,0:T(8,128)(2,1)S(1)} %convolution_convert_fusion.2), channel_id=1, source_target_pairs={{0,1},{1,0},{2,3},{3,2},{4,5},{5,4},{6,7},{7,6},{8,9},{9,8},{10,11... | collective-permute-start | bytes 1572872 | tf_op jit(solution)/shard_map/ppermute | solution.py:40
  63.4 2.0 %collective-permute-start.8 = (bf16[128,2048]{1,0:T(8,128)(2,1)S(1)}, bf16[128,2048]{1,0:T(8,128)(2,1)S(1)}, u32[]{:S(2)}, u32[]{:S(2)}) collective-permute-start(bf16[128,2048]{1,0:T(8,128)(2,1)S(1)} %convolution_convert_fusion.1), channel_id=1, source_target_pairs={{0,1},{1,0},{2,3},{3,2},{4,5},{5,4},{6,7},{7,6},{8,9},{9,8},{10,11... | collective-permute-start | bytes 1572872 | tf_op jit(solution)/shard_map/ppermute | solution.py:40
  65.8 14.0 %collective-permute-start.9 = (bf16[128,2048]{1,0:T(8,128)(2,1)S(1)}, bf16[128,2048]{1,0:T(8,128)(2,1)S(1)}, u32[]{:S(2)}, u32[]{:S(2)}) collective-permute-start(bf16[128,2048]{1,0:T(8,128)(2,1)S(1)} %add_convert_fusion.1), channel_id=1, source_target_pairs={{0,2},{1,3},{2,0},{3,1},{4,6},{5,7},{6,4},{7,5},{8,10},{9,11},{10,... | collective-permute-start | bytes 1572872 | tf_op jit(solution)/shard_map/ppermute | solution.py:40
